TPU v7x, 256 devices: a 8x8x2 block of a 8x8x16 slice. The times are simulated.
256 devices in a mesh: grp: 2 (over z), st: 16 (over y, core), tp: 8 (over x).
Axes of the slice: x: 8, y: 8, z: 2, core: 2. Of those that a mesh axis runs over, the one named last changes fastest.
The devices are a block of a 8x8x16 slice.
Arguments:
- tokens: bfloat16 [8192, 2048], P(('grp', 'st')), parts along dimension 0, may hold values from -6 to 6
- pre_gain: float32 [2048], replicated, may hold values from 0.1 to 1.9
- w_gated: bfloat16 [2048, 1536], P(None, 'tp'), may hold values from -0.125 to 0.125
- w_mixed: bfloat16 [2048, 1536], P(None, 'tp'), may hold values from -0.125 to 0.125
- mix_weight: bfloat16 [8, 128, 128], P('tp'), may hold values from -0.5 to 0.5
- w_query: bfloat16 [2048, 1024], P(None, 'tp'), may hold values from -0.125 to 0.125
- w_gate_mix: bfloat16 [2048, 1536], P(None, 'tp'), may hold values from -0.125 to 0.125
- w_gate_read: bfloat16 [2048, 1024], P(None, 'tp'), may hold values from -0.125 to 0.125
- store: bfloat16 [256, 128, 2048], P(('grp', 'st')), parts along dimension 0, may hold values from -6 to 6
- mem_gain: float32 [2048], replicated, may hold values from 1 to 80
- w_key: bfloat16 [2048, 1024], P(None, 'tp'), may hold values from -0.125 to 0.125
- w_value: bfloat16 [2048, 1024], P(None, 'tp'), may hold values from -0.125 to 0.125
- passage_ids: int32 [128, 4], P(('grp', 'st')), parts along dimension 0, may hold values from 0 to 127, as said below
- w_out_mix: bfloat16 [1536, 2048], P('tp'), may hold values from -0.125 to 0.125
- w_out_read: bfloat16 [1024, 2048], P('tp'), may hold values from -0.125 to 0.125
Outputs:
- mixed_out: bfloat16 [8192, 2048], P(('grp', 'st', 'tp')), parts along dimension 0
There are 2 independent parts, one for each index of `grp`. A program takes and returns all parts, laid end to end along the dimension named above; an argument that names none is the same for every part. Nothing has to cross between parts.
Inputs may be any that keep to these rules, and one draw needn't show every extreme that they name: `passage_ids`: passage p is held by index p // 8 of st. The 16 entries of one index of st name at most 2 passages held by any one index of st, and that most is reached in every draw.
All inputs are finite; a program needn't handle non-finite values.
Results may differ from a plain program's by a relative error of at most 0.015.
The roundings to bfloat16 on the way count: a program that leaves them out, or rounds other values in their place, can miss the bound.
Values may be sent and summed in bfloat16 or wider, within the bound.
A program may use at most 128 MiB of HBM per device.

v0:
```python
import jax
import jax.numpy as jnp
from jax import lax
from jax.sharding import PartitionSpec as P

HD = 128
SPAN = 128
RBLOCK = 64
NPB = 4
PROWS = 128
eps = 1e-06


def split_up(x, dim, size):
    lengths = x.shape
    parts = x.reshape(*lengths[:dim], size, lengths[dim] // size, *lengths[dim + 1 :])
    return jnp.moveaxis(parts, dim, 0)


def summed_on_arrival(x, axis, dim):
    parts = split_up(x, dim, lax.axis_size(axis))
    arrived = lax.all_to_all(parts, axis, split_axis=0, concat_axis=0, tiled=True)
    return arrived.astype(jnp.float32).sum(axis=0)


def row_norm(values_in, gain):
    widened = values_in.astype(jnp.float32)
    return (
        widened * lax.rsqrt(jnp.mean(widened * widened, axis=-1, keepdims=True) + eps) * gain
    ).astype(jnp.bfloat16)


def local(
    tokens,
    pre_gain,
    w_gated,
    w_mixed,
    mix_weight,
    w_query,
    w_gate_mix,
    w_gate_read,
    store,
    mem_gain,
    w_key,
    w_value,
    passage_ids,
    w_out_mix,
    w_out_read,
):
    tok_rows = tokens.shape[0]
    st_count = lax.axis_size("st")
    normed = row_norm(tokens, pre_gain)
    gated = jnp.dot(normed, w_gated, preferred_element_type=jnp.float32)
    mixed_in = jnp.dot(normed, w_mixed, preferred_element_type=jnp.float32)
    groups_here = mix_weight.shape[0]
    group_width = mixed_in.shape[1] // groups_here
    grouped = mixed_in.reshape(tok_rows, groups_here, group_width)
    group_mean = jnp.mean(grouped, axis=-1, keepdims=True)
    centred = grouped - group_mean
    group_var = jnp.mean(centred * centred, axis=-1, keepdims=True)
    mixed_norm = (centred * lax.rsqrt(group_var + eps)).astype(jnp.bfloat16)
    causal = jnp.tril(jnp.ones((SPAN, SPAN), dtype=bool))
    mix_masked = jnp.where(causal[None], mix_weight, jnp.zeros_like(mix_weight))
    blocked = mixed_norm.reshape(tok_rows // SPAN, SPAN, groups_here, group_width)
    spatial = jnp.einsum(
        "hts,nshd->nthd", mix_masked, blocked, preferred_element_type=jnp.float32
    ).reshape(tok_rows, -1)
    branch_mix = gated * spatial
    query = jnp.dot(normed, w_query, preferred_element_type=jnp.float32).astype(jnp.bfloat16)
    head_width = w_query.shape[1]
    heads_here = head_width // HD
    flat_ids = passage_ids.reshape(-1)
    req_count = flat_ids.shape[0]
    per_owner = store.shape[0]
    capacity = max(2, (2 * req_count + st_count - 1) // st_count)
    owner = flat_ids // per_owner
    local_id = flat_ids - owner * per_owner
    position = jnp.arange(req_count, dtype=jnp.int32)
    same_owner = owner[:, None] == owner[None, :]
    earlier = position[None, :] < position[:, None]
    rank = jnp.sum((same_owner & earlier).astype(jnp.int32), axis=1)
    slot = owner * capacity + rank
    slot_range = jnp.arange(st_count * capacity, dtype=jnp.int32)
    table = jnp.sum(jnp.where(slot[:, None] == slot_range[None, :], local_id[:, None], 0), axis=0)
    table = table.reshape(st_count, capacity)
    held_rows = row_norm(store, mem_gain).reshape(-1, store.shape[-1])
    key_store = (
        jnp.dot(held_rows, w_key, preferred_element_type=jnp.float32)
        .astype(jnp.bfloat16)
        .reshape(per_owner, PROWS, head_width)
    )
    value_store = (
        jnp.dot(held_rows, w_value, preferred_element_type=jnp.float32)
        .astype(jnp.bfloat16)
        .reshape(per_owner, PROWS, head_width)
    )
    wanted = lax.all_to_all(table, "st", split_axis=0, concat_axis=0, tiled=True)
    arrived = (
        lax.all_to_all(key_store[wanted], "st", split_axis=0, concat_axis=0, tiled=True),
        lax.all_to_all(value_store[wanted], "st", split_axis=0, concat_axis=0, tiled=True),
    )
    blocks_here = tok_rows // RBLOCK
    key_slots, value_slots = arrived
    keys = key_slots.reshape(st_count * capacity, PROWS, head_width)[slot]
    values = value_slots.reshape(st_count * capacity, PROWS, head_width)[slot]
    keys = keys.reshape(blocks_here, NPB * PROWS, heads_here, HD)
    values = values.reshape(blocks_here, NPB * PROWS, heads_here, HD)
    query_blocks = query.reshape(blocks_here, RBLOCK, heads_here, HD)
    scores = jnp.einsum(
        "btha,bkha->bhtk", query_blocks, keys, preferred_element_type=jnp.float32
    ) * HD ** (-0.5)
    probs = jax.nn.softmax(scores, axis=-1).astype(jnp.bfloat16)
    branch_read = jnp.einsum(
        "bhtk,bkha->btha", probs, values, preferred_element_type=jnp.float32
    ).reshape(tok_rows, head_width)
    gate_mix = jnp.dot(normed, w_gate_mix, preferred_element_type=jnp.float32)
    gate_read = jnp.dot(normed, w_gate_read, preferred_element_type=jnp.float32)
    out_mix = (branch_mix * jax.nn.silu(gate_mix)).astype(jnp.bfloat16)
    out_read = (branch_read * jax.nn.silu(gate_read)).astype(jnp.bfloat16)
    summed = summed_on_arrival(
        (
            jnp.dot(out_mix, w_out_mix, preferred_element_type=jnp.float32)
            + jnp.dot(out_read, w_out_read, preferred_element_type=jnp.float32)
        ).astype(jnp.bfloat16),
        "tp",
        0,
    )
    return summed.astype(jnp.bfloat16)


def solution(mesh):
    placed = (
        P(("grp", "st"), None),
        P(),
        P(None, "tp"),
        P(None, "tp"),
        P("tp", None, None),
        P(None, "tp"),
        P(None, "tp"),
        P(None, "tp"),
        P(("grp", "st"), None, None),
        P(),
        P(None, "tp"),
        P(None, "tp"),
        P(("grp", "st"), None),
        P("tp", None),
        P("tp", None),
    )
    return jax.shard_map(
        local, mesh=mesh, in_specs=placed, out_specs=P(("grp", "st", "tp"), None), check_vma=False
    )
```

profile of v0, /device:TPU:513, one launch (start us, length us, event | category | flops | bytes accessed | tf_op | source)
XLA Modules:
  0.0 140.8 jit_solution(3696719735241878890)
XLA Ops:
  0.0 0.0 copy-start
  0.0 0.8 reshape.317
  0.9 0.2 convert_reduce_fusion
  1.0 0.1 select_reduce_fusion
  1.1 0.7 all_to_all.17
  1.8 23.7 %all-to-all-start = ((s32[16,1,2]{2,1,0:T(1,128)}), s32[16,1,2]{2,1,0:T(1,128)S(1)}, u32[]{:S(2)}, u32[]{:S(2)}) async-start(s32[16,1,2]{2,1,0:T(1,128)} %bitcast.6), calls=%async_computation | async-start | bytes 16384 | tf_op jit(solution)/shard_map/all_to_all | solution.py:97
  25.5 0.0 copy-start.1
  25.5 0.0 copy-start.7
  25.5 3.2 %fusion.1 = f32[8,128]{1,0:T(8,128)S(1)} fusion(bf16[8,128,2048]{2,1,0:T(8,128)(2,1)} %param.23), kind=kLoop, calls=%fused_computation.7 | loop fusion | flops 6290432 | bytes 4198400 | tf_op jit(solution)/shard_map/reduce_sum | solution.py:29
  28.8 0.2 copy-done.1
  29.0 0.0 copy-done.7
  29.0 0.0 copy-start.11
  29.0 1.0 fusion.3
  30.0 0.0 copy-start.2
  30.0 1.9 %copy-done.2 = bf16[8,128,2048]{2,1,0:T(8,128)(2,1)} copy-done((bf16[8,128,2048]{2,1,0:T(8,128)(2,1)}, bf16[8,128,2048]{2,1,0:T(8,128)(2,1)S(1)}, u32[]{:S(2)}) %copy-start.2) | copy-done | bytes 4194328
  31.9 0.0 copy-done.11
  31.9 1.2 convolution_convert_fusion
  33.2 0.0 all-to-all-done
  33.2 0.1 copy.31
  33.3 0.1 copy.32
  33.4 0.1 reshape.329
  33.5 0.0 copy-start.9
  33.5 0.0 copy-start.3
  33.5 1.7 %gather_fusion.2 = bf16[32,128,128]{2,1,0:T(8,128)(2,1)} fusion(bf16[8,128,128]{2,1,0:T(8,128)(2,1)S(1)} %bitcast.74, s32[1024]{0:T(1024)S(1)} %pad_clamp_fusion.1), kind=kCustom, calls=%fused_computation.2 | custom fusion | bytes 2097280 | tf_op jit(solution)/shard_map/gather | solution.py:99
  35.1 0.0 copy-start.8
  35.2 7.5 %all-to-all-start.2 = ((bf16[16,2,128,128]{3,2,1,0:T(8,128)(2,1)}), bf16[16,2,128,128]{3,2,1,0:T(8,128)(2,1)S(1)}, u32[]{:S(2)}, u32[]{:S(2)}) async-start(bf16[16,2,128,128]{3,2,1,0:T(8,128)(2,1)} %bitcast.15), calls=%async_computation.2 | async-start | bytes 2097152 | tf_op jit(solution)/shard_map/all_to_all | solution.py:99
  42.7 0.0 copy-done.9
  42.7 0.1 reshape.319
  42.7 0.0 copy-done.3
  42.7 0.0 copy-start.12
  42.7 0.3 fusion.5
  43.0 0.0 copy-done.8
  43.1 1.7 %fusion.46 = (f32[256]{0:T(256)S(1)}, f32[256,192]{0,1:T(8,128)S(1)}) fusion(bf16[2048,192]{0,1:T(8,128)(2,1)} %param.18, bf16[256,2048]{1,0:T(8,128)(2,1)S(1)} %copy-done.3, f32[2048]{0:T(1024)S(1)} %copy-done.8, f32[256]{0:T(256)S(1)} %add_rsqrt_fusion.2), kind=kOutput, calls=%fused_computation.80 | convolution fusion | flops 203472640 | bytes 2041856 | tf_op jit(solution)/shard_map/dot_general | solution.py:54
  44.8 0.0 copy-done.12
  44.8 3.4 %convolution_convert_fusion.1 = bf16[1024,128]{1,0:T(8,128)(2,1)S(1)} fusion(bf16[1024,2048]{1,0:T(8,128)(2,1)} %bitcast.73, bf16[2048,128]{1,0:T(8,128)(2,1)S(1)} %copy-done.12), kind=kOutput, calls=%fused_computation.21 | convolution fusion | flops 537001984 | bytes 4980736 | tf_op jit(solution)/shard_map/dot_general | solution.py:93
  48.3 0.0 copy-start.6
  48.3 1.7 %gather_fusion = bf16[32,128,128]{2,1,0:T(8,128)(2,1)} fusion(bf16[8,128,128]{2,1,0:T(8,128)(2,1)S(1)} %bitcast.75, s32[1024]{0:T(1024)S(1)} %pad_clamp_fusion.1), kind=kCustom, calls=%fused_computation | custom fusion | bytes 2097280 | tf_op jit(solution)/shard_map/gather | solution.py:100
  50.0 20.7 %all-to-all-done.2 = bf16[16,2,128,128]{3,2,1,0:T(8,128)(2,1)S(1)} async-done(((bf16[16,2,128,128]{3,2,1,0:T(8,128)(2,1)}), bf16[16,2,128,128]{3,2,1,0:T(8,128)(2,1)S(1)}, u32[]{:S(2)}, u32[]{:S(2)}) %all-to-all-start.2) | async-done | bytes 1048608 | tf_op jit(solution)/shard_map/all_to_all | solution.py:99
  70.6 0.0 copy-start.4
  70.6 4.4 %all-to-all-start.1 = ((bf16[16,2,128,128]{3,2,1,0:T(8,128)(2,1)}), bf16[16,2,128,128]{3,2,1,0:T(8,128)(2,1)}, u32[]{:S(2)}, u32[]{:S(2)}) async-start(bf16[16,2,128,128]{3,2,1,0:T(8,128)(2,1)} %bitcast.8), calls=%async_computation.1 | async-start | bytes 2097152 | tf_op jit(solution)/shard_map/all_to_all | solution.py:100
  75.1 0.0 copy-start.10
  75.1 0.0 copy-done.6
  75.1 0.2 convolution_bitcast_fusion
  75.3 0.2 copy.29
  75.5 2.2 %convolution_convert_fusion.2 = bf16[256,128]{1,0:T(8,128)(2,1)} fusion(bf16[2048,128]{1,0:T(8,128)(2,1)} %param.20, bf16[256,2048]{1,0:T(8,128)(2,1)S(1)} %copy-done.3, f32[2048]{0:T(1024)S(1)} %copy-done.8, f32[256]{0:T(256)S(1)} %add_rsqrt_fusion.2), kind=kOutput, calls=%fused_computation.27 | convolution fusion | flops 136347648 | bytes 1647616 | tf_op jit(solution)/shard_map/dot_general | solution.py:69
  77.7 0.0 copy-done.4
  77.7 0.0 copy-done.10
  77.7 0.6 fusion.38
  78.3 0.0 copy-done
  78.3 3.0 %fusion.12 = f32[256,2048]{1,0:T(8,128)S(1)} fusion(bf16[192,2048]{1,0:T(8,128)(2,1)S(1)} %copy-done, bf16[2048,192]{0,1:T(8,128)(2,1)} %param.17, f32[24,8,2,128]{3,2,1,0:T(2,128)S(1)} %bitcast.78, f32[256,192]{0,1:T(8,128)S(1)} %fusion.38, bf16[256,2048]{1,0:T(8,128)(2,1)} %param.15, f32[2048]{0:T(1024)S(1)} %copy-done.8, f32[256]{0:T(256)S(1)} %add_rsqrt_fusion.2), kind=kOutput, calls=%fused_computation.26 | convolution fusion | flops 405094400 | bytes 5121024 | tf_op jit(solution)/shard_map/dot_general | solution.py:122
  81.2 2.6 %gather_fusion.3 = bf16[16,128,128]{2,1,0:T(8,128)(2,1)} fusion(bf16[32,128,128]{2,1,0:T(8,128)(2,1)} %bitcast.76, s32[1024]{0:T(1024)S(1)} %pad_clamp_fusion), kind=kCustom, calls=%fused_computation.3 | custom fusion | bytes 1048640 | tf_op jit(solution)/shard_map/gather | solution.py:104
  83.9 1.4 convolution_multiply_fusion
  85.2 0.2 fusion.47
  85.5 16.7 %all-to-all-done.1 = bf16[16,2,128,128]{3,2,1,0:T(8,128)(2,1)} async-done(((bf16[16,2,128,128]{3,2,1,0:T(8,128)(2,1)}), bf16[16,2,128,128]{3,2,1,0:T(8,128)(2,1)}, u32[]{:S(2)}, u32[]{:S(2)}) %all-to-all-start.1) | async-done | bytes 1048608 | tf_op jit(solution)/shard_map/all_to_all | solution.py:100
  102.1 2.6 %gather_fusion.1 = bf16[16,128,128]{2,1,0:T(8,128)(2,1)} fusion(bf16[32,128,128]{2,1,0:T(8,128)(2,1)} %bitcast.9, s32[1024]{0:T(1024)S(1)} %pad_clamp_fusion), kind=kCustom, calls=%fused_computation.1 | custom fusion | bytes 1048640 | tf_op jit(solution)/shard_map/gather | solution.py:105
  104.8 2.3 %fusion.13 = f32[4,128,64]{1,2,0:T(8,128)} fusion(bf16[4,512,128]{2,1,0:T(8,128)(2,1)} %bitcast.79, f32[4,64]{1,0:T(4,128)S(1)} %fusion.47, f32[4,64,512]{2,1,0:T(8,128)S(1)} %convolution_multiply_fusion), kind=kOutput, calls=%fused_computation.29 | convolution fusion | flops 33948416 | bytes 1180672 | tf_op jit(solution)/shard_map/bhtk,bkha->btha/dot_general | solution.py:113
  107.0 0.0 copy-start.5
  107.0 2.0 %fusion.21 = bf16[256,128]{1,0:T(8,128)(2,1)S(1)} fusion(f32[4,128,64]{1,2,0:T(8,128)} %fusion.13, bf16[2048,128]{1,0:T(8,128)(2,1)} %param.22, bf16[256,2048]{1,0:T(8,128)(2,1)} %param.15, f32[2048]{0:T(1024)S(1)} %copy-done.8, f32[256]{0:T(256)S(1)} %add_rsqrt_fusion.2), kind=kOutput, calls=%fused_computation.40 | convolution fusion | flops 136511488 | bytes 1778688 | tf_op jit(solution)/shard_map/dot_general | solution.py:117
  109.0 0.0 copy-done.5
  109.0 0.4 fusion.4
  109.4 30.6 %all_to_all.27 = bf16[8,32,2048]{2,1,0:T(8,128)(2,1)S(1)} all-to-all(bf16[8,32,2048]{2,1,0:T(8,128)(2,1)S(1)} %bitcast.71), channel_id=1, replica_groups=mesh['grp'=2,'st'=16,'tp'=8] {'tp'}, dimensions={0} | all-to-all | bytes 2097152 | tf_op jit(solution)/shard_map/all_to_all | solution.py:22
  140.0 0.8 reduce_sum.85
  (11 shorter events, 0.1 us)
Async XLA Ops:
  0.0 78.3 %copy-start = (bf16[192,2048]{1,0:T(8,128)(2,1)S(1)}, bf16[192,2048]{1,0:T(8,128)(2,1)}, u32[]{:S(2)}) copy-start(bf16[192,2048]{1,0:T(8,128)(2,1)} %param.28) | copy-start | bytes 2359300
  1.8 31.4 %all-to-all-start = ((s32[16,1,2]{2,1,0:T(1,128)}), s32[16,1,2]{2,1,0:T(1,128)S(1)}, u32[]{:S(2)}, u32[]{:S(2)}) async-start(s32[16,1,2]{2,1,0:T(1,128)} %bitcast.6), calls=%async_computation | async-start | bytes 16384 | tf_op jit(solution)/shard_map/all_to_all | solution.py:97
  25.5 3.4 %copy-start.1 = (bf16[8,128,2048]{2,1,0:T(8,128)(2,1)S(1)}, bf16[8,128,2048]{2,1,0:T(8,128)(2,1)}, u32[]{:S(2)}) copy-start(bf16[8,128,2048]{2,1,0:T(8,128)(2,1)} %param.23) | copy-start | bytes 12582916
  25.5 3.4 %copy-start.7 = (f32[2048]{0:T(1024)S(1)}, f32[2048]{0:T(1024)}, u32[]{:S(2)}) copy-start(f32[2048]{0:T(1024)} %param.24) | copy-start | bytes 24580
  29.0 3.0 %copy-start.11 = (bf16[2048,128]{1,0:T(8,128)(2,1)S(1)}, bf16[2048,128]{1,0:T(8,128)(2,1)}, u32[]{:S(2)}) copy-start(bf16[2048,128]{1,0:T(8,128)(2,1)} %param.25) | copy-start | bytes 1572868
  30.0 1.9 %copy-start.2 = (bf16[8,128,2048]{2,1,0:T(8,128)(2,1)}, bf16[8,128,2048]{2,1,0:T(8,128)(2,1)S(1)}, u32[]{:S(2)}) copy-start(bf16[8,128,2048]{2,1,0:T(8,128)(2,1)S(1)} %fusion.3) | copy-start | bytes 12582916
  33.5 9.2 %copy-start.9 = (s32[4,4]{1,0:T(4,128)S(1)}, s32[4,4]{1,0:T(4,128)}, u32[]{:S(2)}) copy-start(s32[4,4]{1,0:T(4,128)} %param.27) | copy-start | bytes 196
  33.5 9.3 %copy-start.3 = (bf16[256,2048]{1,0:T(8,128)(2,1)S(1)}, bf16[256,2048]{1,0:T(8,128)(2,1)}, u32[]{:S(2)}) copy-start(bf16[256,2048]{1,0:T(8,128)(2,1)} %param.15) | copy-start | bytes 3145732
  35.1 7.9 %copy-start.8 = (f32[2048]{0:T(1024)S(1)}, f32[2048]{0:T(1024)}, u32[]{:S(2)}) copy-start(f32[2048]{0:T(1024)} %param.16) | copy-start | bytes 24580
  35.2 35.5 %all-to-all-start.2 = ((bf16[16,2,128,128]{3,2,1,0:T(8,128)(2,1)}), bf16[16,2,128,128]{3,2,1,0:T(8,128)(2,1)S(1)}, u32[]{:S(2)}, u32[]{:S(2)}) async-start(bf16[16,2,128,128]{3,2,1,0:T(8,128)(2,1)} %bitcast.15), calls=%async_computation.2 | async-start | bytes 2097152 | tf_op jit(solution)/shard_map/all_to_all | solution.py:99
  42.7 2.1 %copy-start.12 = (bf16[2048,128]{1,0:T(8,128)(2,1)S(1)}, bf16[2048,128]{1,0:T(8,128)(2,1)}, u32[]{:S(2)}) copy-start(bf16[2048,128]{1,0:T(8,128)(2,1)} %param.26) | copy-start | bytes 1572868
  48.3 26.8 %copy-start.6 = (bf16[1,128,128]{2,1,0:T(8,128)(2,1)S(1)}, bf16[1,128,128]{2,1,0:T(8,128)(2,1)}, u32[]{:S(2)}) copy-start(bf16[1,128,128]{2,1,0:T(8,128)(2,1)} %param.19) | copy-start | bytes 98308
  70.6 7.0 %copy-start.4 = (bf16[16,2,128,128]{3,2,1,0:T(8,128)(2,1)}, bf16[16,2,128,128]{3,2,1,0:T(8,128)(2,1)S(1)}, u32[]{:S(2)}) copy-start(bf16[16,2,128,128]{3,2,1,0:T(8,128)(2,1)S(1)} %all-to-all-done.2) | copy-start | bytes 3145732
  70.6 31.5 %all-to-all-start.1 = ((bf16[16,2,128,128]{3,2,1,0:T(8,128)(2,1)}), bf16[16,2,128,128]{3,2,1,0:T(8,128)(2,1)}, u32[]{:S(2)}, u32[]{:S(2)}) async-start(bf16[16,2,128,128]{3,2,1,0:T(8,128)(2,1)} %bitcast.8), calls=%async_computation.1 | async-start | bytes 2097152 | tf_op jit(solution)/shard_map/all_to_all | solution.py:100
  75.1 2.6 %copy-start.10 = (bf16[2048,192]{0,1:T(8,128)(2,1)S(1)}, bf16[2048,192]{0,1:T(8,128)(2,1)}, u32[]{:S(2)}) copy-start(bf16[2048,192]{0,1:T(8,128)(2,1)} %param.21) | copy-start | bytes 2359300
  107.0 2.0 %copy-start.5 = (bf16[128,2048]{1,0:T(8,128)(2,1)S(1)}, bf16[128,2048]{1,0:T(8,128)(2,1)}, u32[]{:S(2)}) copy-start(bf16[128,2048]{1,0:T(8,128)(2,1)} %param.29) | copy-start | bytes 1572868
where the time goes:
time: 141 us
  waiting for transfers between devices  37.3 us (26%)
  starting transfers between devices  35.6 us (25%)
  blocking collectives  30.6 us (22%)
  matrix products  18.3 us (13%)
  local copies, waits for them, and re-layouts  12.8 us (9%)
  other arithmetic  5.97 us (4%)
    all_to_all x1, blocking collectives, summed_on_arrival(): lax.all_to_all(parts, axis, split_axis=0, concat_axis=0, tiled=True)  30.6 us
    all_to_all x1, starting transfers between devices, local(): lax.all_to_all(table, 'st', split_axis=0, concat_axis=0, tiled=True)  23.7 us
    all_to_all x1, waiting for transfers between devices, local(): lax.all_to_all(key_store[wanted], 'st', split_axis=0, concat_axis=0, tile...  20.7 us
    all_to_all x1, waiting for transfers between devices, local(): lax.all_to_all(value_store[wanted], 'st', split_axis=0, concat_axis=0, ti...  16.7 us
    all_to_all x1, starting transfers between devices, local(): lax.all_to_all(key_store[wanted], 'st', split_axis=0, concat_axis=0, tile...  7.5 us
    all_to_all x1, starting transfers between devices, local(): lax.all_to_all(value_store[wanted], 'st', split_axis=0, concat_axis=0, ti...  4.44 us
    reduce_sum x2, other arithmetic, row_norm(): jnp.mean(widened * widened, axis=-1, keepdims=True) + eps  3.51 us
    dot_general x1, matrix products, local(): jnp.dot(held_rows, w_value, preferred_element_type=jnp.float32)  3.44 us
  transfers between devices with their start and end apart: 3, of which 2 were waited for; matrix products, arithmetic and copies ran while one was open for 16% of the time, Pallas kernels for 0%

commit v1 on v0

--- a/solution.py
+++ b/solution.py
@@ -9,6 +9,22 @@
 NPB = 4
 PROWS = 128
 eps = 1e-06
+
+
+def swapped_with_each(value, axis, split, join):
+    ways, here = (lax.axis_size(axis), lax.axis_index(axis))
+    width = value.shape[split] // ways
+    shape = list(value.shape)
+    shape[split] = width
+    height = shape[join]
+    shape[join] = height * ways
+    full = jnp.zeros(shape, value.dtype)
+    for mask in range(ways):
+        part = lax.dynamic_slice_in_dim(value, (here ^ mask) * width, width, axis=split)
+        if mask:
+            part = lax.ppermute(part, axis, [(d, d ^ mask) for d in range(ways)])
+        full = lax.dynamic_update_slice_in_dim(full, part, (here ^ mask) * height, axis=join)
+    return full
 
 
 def split_up(x, dim, size):
@@ -94,7 +110,7 @@
         .astype(jnp.bfloat16)
         .reshape(per_owner, PROWS, head_width)
     )
-    wanted = lax.all_to_all(table, "st", split_axis=0, concat_axis=0, tiled=True)
+    wanted = swapped_with_each(table, "st", 0, 0)
     arrived = (
         lax.all_to_all(key_store[wanted], "st", split_axis=0, concat_axis=0, tiled=True),
         lax.all_to_all(value_store[wanted], "st", split_axis=0, concat_axis=0, tiled=True),

time: 141 us -> 164 us (1.16)
  starting transfers between devices: 35.6 us -> 56.7 us
  other arithmetic: 5.97 us -> 8.07 us
  local copies, waits for them, and re-layouts: 12.8 us -> 11.1 us
    ppermute x0 -> x15, starting transfers between devices: none -> 46.9 us  [swapped_with_each(): part = lax.ppermute(part, axis, [(d, d ^ mask) for d in range(ways)])]
    all_to_all x1 -> x0, starting transfers between devices: 23.7 us -> none  [local(): lax.all_to_all(table, 'st', split_axis=0, concat_axis=0, tiled=True)]
    convert_element_type x1, other arithmetic: 1.02 us -> 3.27 us  [row_norm(): return (widened * lax.rsqrt(jnp.mean(widened * widened, axis=-1, keepdims...]
    all_to_all x1, starting transfers between devices: 7.5 us -> 5.38 us  [local(): lax.all_to_all(key_store[wanted], 'st', split_axis=0, concat_axis=0, tile...]
  transfers between devices with their start and end apart: 3 -> 17, of which waited for: 2 -> 4; matrix products, arithmetic and copies ran while one was open for 16% -> 16% of each run, Pallas kernels for 0% -> 0%
where the time goes in v1:
time: 164 us
  starting transfers between devices  56.7 us (35%)
  waiting for transfers between devices  38.5 us (23%)
  blocking collectives  30.6 us (19%)
  matrix products  18.3 us (11%)
  local copies, waits for them, and re-layouts  11.1 us (7%)
  other arithmetic  8.07 us (5%)
    ppermute x15, starting transfers between devices, swapped_with_each(): part = lax.ppermute(part, axis, [(d, d ^ mask) for d in range(ways)])  46.9 us
    all_to_all x1, blocking collectives, summed_on_arrival(): lax.all_to_all(parts, axis, split_axis=0, concat_axis=0, tiled=True)  30.6 us
    all_to_all x1, waiting for transfers between devices, local(): lax.all_to_all(key_store[wanted], 'st', split_axis=0, concat_axis=0, tile...  20.7 us
    all_to_all x1, waiting for transfers between devices, local(): lax.all_to_all(value_store[wanted], 'st', split_axis=0, concat_axis=0, ti...  16.6 us
    all_to_all x1, starting transfers between devices, local(): lax.all_to_all(key_store[wanted], 'st', split_axis=0, concat_axis=0, tile...  5.38 us
    all_to_all x1, starting transfers between devices, local(): lax.all_to_all(value_store[wanted], 'st', split_axis=0, concat_axis=0, ti...  4.45 us
    dot_general x1, matrix products, local(): jnp.dot(held_rows, w_value, preferred_element_type=jnp.float32)  3.44 us
    reduce_sum x2, other arithmetic, row_norm(): jnp.mean(widened * widened, axis=-1, keepdims=True) + eps  3.36 us
  transfers between devices with their start and end apart: 17, of which 4 were waited for; matrix products, arithmetic and copies ran while one was open for 16% of the time, Pallas kernels for 0%

profile of v1, /device:TPU:513, one launch (start us, length us, event | category | flops | bytes accessed | tf_op | source)
XLA Modules:
  0.0 163.6 jit_solution(18165602198646006598)
XLA Ops:
  0.0 0.8 reshape.288
  0.9 0.2 convert_reduce_fusion
  1.0 0.1 select_reduce_fusion
  1.1 0.1 reshape.289
  1.3 0.1 constant_dynamic-slice_fusion
  1.4 20.5 %collective-permute-start = (s32[1,2]{1,0:T(1,128)S(1)}, s32[1,2]{1,0:T(1,128)S(1)}, u32[]{:S(2)}, u32[]{:S(2)}) collective-permute-start(s32[1,2]{1,0:T(1,128)S(1)} %get-tuple-element.21), channel_id=1, source_target_pairs={{0,8},{8,0},{16,24},{24,16},{32,40},{40,32},{48,56},{56,48},{64,72... | collective-permute-start | bytes 32 | tf_op jit(solution)/shard_map/ppermute | solution.py:25
  21.9 0.0 collective-permute-start.1
  21.9 1.8 %collective-permute-start.2 = (s32[1,2]{1,0:T(1,128)S(1)}, s32[1,2]{1,0:T(1,128)S(1)}, u32[]{:S(2)}, u32[]{:S(2)}) collective-permute-start(s32[1,2]{1,0:T(1,128)S(1)} %get-tuple-element.19), channel_id=1, source_target_pairs={{0,24},{8,16},{16,8},{24,0},{32,56},{40,48},{48,40},{56,32},{64,88... | collective-permute-start | bytes 32 | tf_op jit(solution)/shard_map/ppermute | solution.py:25
  23.7 0.0 collective-permute-start.3
  23.7 2.6 %collective-permute-start.4 = (s32[1,2]{1,0:T(1,128)S(1)}, s32[1,2]{1,0:T(1,128)S(1)}, u32[]{:S(2)}, u32[]{:S(2)}) collective-permute-start(s32[1,2]{1,0:T(1,128)S(1)} %get-tuple-element.17), channel_id=1, source_target_pairs={{0,40},{8,32},{16,56},{24,48},{32,8},{40,0},{48,24},{56,16},{64,10... | collective-permute-start | bytes 32 | tf_op jit(solution)/shard_map/ppermute | solution.py:25
  26.3 3.1 %fusion.1 = f32[8,128]{1,0:T(8,128)S(1)} fusion(bf16[8,128,2048]{2,1,0:T(8,128)(2,1)} %param.23), kind=kLoop, calls=%fused_computation.7 | loop fusion | flops 6290432 | bytes 4198400 | tf_op jit(solution)/shard_map/reduce_sum | solution.py:45
  29.4 0.0 copy-start.10
  29.4 3.3 %fusion.3 = bf16[8,128,2048]{2,1,0:T(8,128)(2,1)S(1)} fusion(bf16[8,128,2048]{2,1,0:T(8,128)(2,1)} %param.23, f32[2048]{0:T(1024)S(1)} %copy-done.6, f32[8,128]{1,0:T(8,128)S(1)} %add_rsqrt_fusion), kind=kLoop, calls=%fused_computation.9 | loop fusion | flops 8388608 | bytes 8400896 | tf_op jit(solution)/shard_map/convert_element_type | solution.py:46
  32.7 1.2 convolution_convert_fusion
  34.0 0.7 copy-done.1
  34.7 0.0 collective-permute-done
  34.7 0.0 collective-permute-start.5
  34.7 0.0 collective-permute-done.1
  34.7 3.7 %collective-permute-start.6 = (s32[1,2]{1,0:T(1,128)S(1)}, s32[1,2]{1,0:T(1,128)S(1)}, u32[]{:S(2)}, u32[]{:S(2)}) collective-permute-start(s32[1,2]{1,0:T(1,128)S(1)} %get-tuple-element.15), channel_id=1, source_target_pairs={{0,56},{8,48},{16,40},{24,32},{32,24},{40,16},{48,8},{56,0},{64,12... | collective-permute-start | bytes 32 | tf_op jit(solution)/shard_map/ppermute | solution.py:25
  38.4 0.0 collective-permute-done.2
  38.4 0.1 collective-permute-start.7
  38.6 5.7 %collective-permute-start.8 = (s32[1,2]{1,0:T(1,128)S(1)}, s32[1,2]{1,0:T(1,128)S(1)}, u32[]{:S(2)}, u32[]{:S(2)}) collective-permute-start(s32[1,2]{1,0:T(1,128)S(1)} %get-tuple-element.13), channel_id=1, source_target_pairs={{0,72},{8,64},{16,88},{24,80},{32,104},{40,96},{48,120},{56,112},{... | collective-permute-start | bytes 32 | tf_op jit(solution)/shard_map/ppermute | solution.py:25
  44.3 0.0 collective-permute-done.4
  44.3 0.1 collective-permute-start.9
  44.5 0.0 collective-permute-done.5
  44.5 4.9 %collective-permute-start.10 = (s32[1,2]{1,0:T(1,128)S(1)}, s32[1,2]{1,0:T(1,128)S(1)}, u32[]{:S(2)}, u32[]{:S(2)}) collective-permute-start(s32[1,2]{1,0:T(1,128)S(1)} %get-tuple-element.11), channel_id=1, source_target_pairs={{0,88},{8,80},{16,72},{24,64},{32,120},{40,112},{48,104},{56,96},{... | collective-permute-start | bytes 32 | tf_op jit(solution)/shard_map/ppermute | solution.py:25
  49.4 0.0 collective-permute-done.6
  49.4 0.1 collective-permute-start.11
  49.6 3.9 %collective-permute-start.12 = (s32[1,2]{1,0:T(1,128)S(1)}, s32[1,2]{1,0:T(1,128)S(1)}, u32[]{:S(2)}, u32[]{:S(2)}) collective-permute-start(s32[1,2]{1,0:T(1,128)S(1)} %get-tuple-element.9), channel_id=1, source_target_pairs={{0,104},{8,96},{16,120},{24,112},{32,72},{40,64},{48,88},{56,80},{... | collective-permute-start | bytes 32 | tf_op jit(solution)/shard_map/ppermute | solution.py:25
  53.5 0.1 collective-permute-start.13
  53.7 0.0 collective-permute-done.9
  53.7 3.2 %collective-permute-start.14 = (s32[1,2]{1,0:T(1,128)S(1)}, s32[1,2]{1,0:T(1,128)S(1)}, u32[]{:S(2)}, u32[]{:S(2)}) collective-permute-start(s32[1,2]{1,0:T(1,128)S(1)} %get-tuple-element.7), channel_id=1, source_target_pairs={{0,120},{8,112},{16,104},{24,96},{32,88},{40,80},{48,72},{56,64},{... | collective-permute-start | bytes 32 | tf_op jit(solution)/shard_map/ppermute | solution.py:25
  57.0 0.0 collective-permute-done.10
  57.1 0.2 collective-permute-done.13
  57.3 0.9 collective-permute-done.14
  58.3 0.1 reshape.301
  58.4 0.0 copy-start.8
  58.4 0.0 copy-start.2
  58.4 1.7 %gather_fusion.2 = bf16[32,128,128]{2,1,0:T(8,128)(2,1)} fusion(bf16[8,128,128]{2,1,0:T(8,128)(2,1)S(1)} %bitcast.69, s32[1024]{0:T(1024)S(1)} %pad_clamp_fusion.1), kind=kCustom, calls=%fused_computation.2 | custom fusion | bytes 2097280 | tf_op jit(solution)/shard_map/gather | solution.py:115
  60.1 5.4 %all-to-all-start.1 = ((bf16[16,2,128,128]{3,2,1,0:T(8,128)(2,1)}), bf16[16,2,128,128]{3,2,1,0:T(8,128)(2,1)S(1)}, u32[]{:S(2)}, u32[]{:S(2)}) async-start(bf16[16,2,128,128]{3,2,1,0:T(8,128)(2,1)} %bitcast.13), calls=%async_computation.1 | async-start | bytes 2097152 | tf_op jit(solution)/shard_map/all_to_all | solution.py:115
  65.4 0.1 reshape.291
  65.5 0.3 fusion.5
  65.8 1.7 %fusion.46 = (f32[256]{0:T(256)S(1)}, f32[256,192]{0,1:T(8,128)S(1)}) fusion(bf16[2048,192]{0,1:T(8,128)(2,1)} %param.18, bf16[256,2048]{1,0:T(8,128)(2,1)S(1)} %copy-done.2, f32[2048]{0:T(1024)S(1)} %copy-done.7, f32[256]{0:T(256)S(1)} %add_rsqrt_fusion.2), kind=kOutput, calls=%fused_computation.96 | convolution fusion | flops 203472640 | bytes 2041856 | tf_op jit(solution)/shard_map/dot_general | solution.py:70
  67.6 3.4 %convolution_convert_fusion.1 = bf16[1024,128]{1,0:T(8,128)(2,1)S(1)} fusion(bf16[1024,2048]{1,0:T(8,128)(2,1)} %bitcast.68, bf16[2048,128]{1,0:T(8,128)(2,1)S(1)} %copy-done.11), kind=kOutput, calls=%fused_computation.21 | convolution fusion | flops 537001984 | bytes 4980736 | tf_op jit(solution)/shard_map/dot_general | solution.py:109
  71.1 0.0 copy-start.5
  71.1 1.6 %gather_fusion = bf16[32,128,128]{2,1,0:T(8,128)(2,1)} fusion(bf16[8,128,128]{2,1,0:T(8,128)(2,1)S(1)} %bitcast.70, s32[1024]{0:T(1024)S(1)} %pad_clamp_fusion.1), kind=kCustom, calls=%fused_computation | custom fusion | bytes 2097280 | tf_op jit(solution)/shard_map/gather | solution.py:116
  72.7 20.7 %all-to-all-done.1 = bf16[16,2,128,128]{3,2,1,0:T(8,128)(2,1)S(1)} async-done(((bf16[16,2,128,128]{3,2,1,0:T(8,128)(2,1)}), bf16[16,2,128,128]{3,2,1,0:T(8,128)(2,1)S(1)}, u32[]{:S(2)}, u32[]{:S(2)}) %all-to-all-start.1) | async-done | bytes 1048608 | tf_op jit(solution)/shard_map/all_to_all | solution.py:115
  93.4 4.4 %all-to-all-start = ((bf16[16,2,128,128]{3,2,1,0:T(8,128)(2,1)}), bf16[16,2,128,128]{3,2,1,0:T(8,128)(2,1)}, u32[]{:S(2)}, u32[]{:S(2)}) async-start(bf16[16,2,128,128]{3,2,1,0:T(8,128)(2,1)} %bitcast.6), calls=%async_computation | async-start | bytes 2097152 | tf_op jit(solution)/shard_map/all_to_all | solution.py:116
  97.9 0.0 copy-start.9
  97.9 0.2 convolution_bitcast_fusion
  98.1 0.2 copy.20
  98.3 2.2 %convolution_convert_fusion.2 = bf16[256,128]{1,0:T(8,128)(2,1)} fusion(bf16[2048,128]{1,0:T(8,128)(2,1)} %param.20, bf16[256,2048]{1,0:T(8,128)(2,1)S(1)} %copy-done.2, f32[2048]{0:T(1024)S(1)} %copy-done.7, f32[256]{0:T(256)S(1)} %add_rsqrt_fusion.2), kind=kOutput, calls=%fused_computation.27 | convolution fusion | flops 136347648 | bytes 1647616 | tf_op jit(solution)/shard_map/dot_general | solution.py:85
  100.5 0.6 fusion.38
  101.1 3.0 %fusion.12 = f32[256,2048]{1,0:T(8,128)S(1)} fusion(bf16[192,2048]{1,0:T(8,128)(2,1)S(1)} %copy-done, bf16[2048,192]{0,1:T(8,128)(2,1)} %param.17, f32[24,8,2,128]{3,2,1,0:T(2,128)S(1)} %bitcast.73, f32[256,192]{0,1:T(8,128)S(1)} %fusion.38, bf16[256,2048]{1,0:T(8,128)(2,1)} %param.15, f32[2048]{0:T(1024)S(1)} %copy-done.7, f32[256]{0:T(256)S(1)} %add_rsqrt_fusion.2), kind=kOutput, calls=%fused_computation.26 | convolution fusion | flops 405094400 | bytes 5121024 | tf_op jit(solution)/shard_map/dot_general | solution.py:138
  104.0 2.6 %gather_fusion.3 = bf16[16,128,128]{2,1,0:T(8,128)(2,1)} fusion(bf16[32,128,128]{2,1,0:T(8,128)(2,1)} %bitcast.71, s32[1024]{0:T(1024)S(1)} %pad_clamp_fusion), kind=kCustom, calls=%fused_computation.3 | custom fusion | bytes 1048640 | tf_op jit(solution)/shard_map/gather | solution.py:120
  106.7 1.4 convolution_multiply_fusion
  108.0 0.2 fusion.47
  108.3 16.6 %all-to-all-done = bf16[16,2,128,128]{3,2,1,0:T(8,128)(2,1)} async-done(((bf16[16,2,128,128]{3,2,1,0:T(8,128)(2,1)}), bf16[16,2,128,128]{3,2,1,0:T(8,128)(2,1)}, u32[]{:S(2)}, u32[]{:S(2)}) %all-to-all-start) | async-done | bytes 1048608 | tf_op jit(solution)/shard_map/all_to_all | solution.py:116
  124.9 2.6 %gather_fusion.1 = bf16[16,128,128]{2,1,0:T(8,128)(2,1)} fusion(bf16[32,128,128]{2,1,0:T(8,128)(2,1)} %bitcast.7, s32[1024]{0:T(1024)S(1)} %pad_clamp_fusion), kind=kCustom, calls=%fused_computation.1 | custom fusion | bytes 1048640 | tf_op jit(solution)/shard_map/gather | solution.py:121
  127.5 2.3 %fusion.13 = f32[4,128,64]{1,2,0:T(8,128)} fusion(bf16[4,512,128]{2,1,0:T(8,128)(2,1)} %bitcast.74, f32[4,64]{1,0:T(4,128)S(1)} %fusion.47, f32[4,64,512]{2,1,0:T(8,128)S(1)} %convolution_multiply_fusion), kind=kOutput, calls=%fused_computation.29 | convolution fusion | flops 33948416 | bytes 1180672 | tf_op jit(solution)/shard_map/bhtk,bkha->btha/dot_general | solution.py:129
  129.8 2.0 %fusion.21 = bf16[256,128]{1,0:T(8,128)(2,1)S(1)} fusion(f32[4,128,64]{1,2,0:T(8,128)} %fusion.13, bf16[2048,128]{1,0:T(8,128)(2,1)} %param.22, bf16[256,2048]{1,0:T(8,128)(2,1)} %param.15, f32[2048]{0:T(1024)S(1)} %copy-done.7, f32[256]{0:T(256)S(1)} %add_rsqrt_fusion.2), kind=kOutput, calls=%fused_computation.40 | convolution fusion | flops 136511488 | bytes 1778688 | tf_op jit(solution)/shard_map/dot_general | solution.py:133
  131.8 0.4 fusion.4
  132.2 30.6 %all_to_all.15 = bf16[8,32,2048]{2,1,0:T(8,128)(2,1)S(1)} all-to-all(bf16[8,32,2048]{2,1,0:T(8,128)(2,1)S(1)} %bitcast.66), channel_id=1, replica_groups=mesh['grp'=2,'st'=16,'tp'=8] {'tp'}, dimensions={0} | all-to-all | bytes 2097152 | tf_op jit(solution)/shard_map/all_to_all | solution.py:38
  162.8 0.8 reduce_sum.85
  (51 shorter events, 0.7 us)
Async XLA Ops:
  0.0 101.1 %copy-start = (bf16[192,2048]{1,0:T(8,128)(2,1)S(1)}, bf16[192,2048]{1,0:T(8,128)(2,1)}, u32[]{:S(2)}) copy-start(bf16[192,2048]{1,0:T(8,128)(2,1)} %param.28) | copy-start | bytes 2359300
  1.4 33.3 %collective-permute-start = (s32[1,2]{1,0:T(1,128)S(1)}, s32[1,2]{1,0:T(1,128)S(1)}, u32[]{:S(2)}, u32[]{:S(2)}) collective-permute-start(s32[1,2]{1,0:T(1,128)S(1)} %get-tuple-element.21), channel_id=1, source_target_pairs={{0,8},{8,0},{16,24},{24,16},{32,40},{40,32},{48,56},{56,48},{64,72... | collective-permute-start | bytes 32 | tf_op jit(solution)/shard_map/ppermute | solution.py:25
  21.9 12.8 %collective-permute-start.1 = (s32[1,2]{1,0:T(1,128)S(1)}, s32[1,2]{1,0:T(1,128)S(1)}, u32[]{:S(2)}, u32[]{:S(2)}) collective-permute-start(s32[1,2]{1,0:T(1,128)S(1)} %get-tuple-element.20), channel_id=1, source_target_pairs={{0,16},{8,24},{16,0},{24,8},{32,48},{40,56},{48,32},{56,40},{64,80... | collective-permute-start | bytes 32 | tf_op jit(solution)/shard_map/ppermute | solution.py:25
  21.9 16.5 %collective-permute-start.2 = (s32[1,2]{1,0:T(1,128)S(1)}, s32[1,2]{1,0:T(1,128)S(1)}, u32[]{:S(2)}, u32[]{:S(2)}) collective-permute-start(s32[1,2]{1,0:T(1,128)S(1)} %get-tuple-element.19), channel_id=1, source_target_pairs={{0,24},{8,16},{16,8},{24,0},{32,56},{40,48},{48,40},{56,32},{64,88... | collective-permute-start | bytes 32 | tf_op jit(solution)/shard_map/ppermute | solution.py:25
  23.7 14.9 %collective-permute-start.3 = (s32[1,2]{1,0:T(1,128)S(1)}, s32[1,2]{1,0:T(1,128)S(1)}, u32[]{:S(2)}, u32[]{:S(2)}) collective-permute-start(s32[1,2]{1,0:T(1,128)S(1)} %get-tuple-element.18), channel_id=1, source_target_pairs={{0,32},{8,40},{16,48},{24,56},{32,0},{40,8},{48,16},{56,24},{64,96... | collective-permute-start | bytes 32 | tf_op jit(solution)/shard_map/ppermute | solution.py:25
  23.7 5.7 %copy-start.6 = (f32[2048]{0:T(1024)S(1)}, f32[2048]{0:T(1024)}, u32[]{:S(2)}) copy-start(f32[2048]{0:T(1024)} %param.24) | copy-start | bytes 24580
  23.7 20.6 %collective-permute-start.4 = (s32[1,2]{1,0:T(1,128)S(1)}, s32[1,2]{1,0:T(1,128)S(1)}, u32[]{:S(2)}, u32[]{:S(2)}) collective-permute-start(s32[1,2]{1,0:T(1,128)S(1)} %get-tuple-element.17), channel_id=1, source_target_pairs={{0,40},{8,32},{16,56},{24,48},{32,8},{40,0},{48,24},{56,16},{64,10... | collective-permute-start | bytes 32 | tf_op jit(solution)/shard_map/ppermute | solution.py:25
  29.4 3.3 %copy-start.10 = (bf16[2048,128]{1,0:T(8,128)(2,1)S(1)}, bf16[2048,128]{1,0:T(8,128)(2,1)}, u32[]{:S(2)}) copy-start(bf16[2048,128]{1,0:T(8,128)(2,1)} %param.25) | copy-start | bytes 1572868
  32.7 1.9 %copy-start.1 = (bf16[8,128,2048]{2,1,0:T(8,128)(2,1)}, bf16[8,128,2048]{2,1,0:T(8,128)(2,1)S(1)}, u32[]{:S(2)}) copy-start(bf16[8,128,2048]{2,1,0:T(8,128)(2,1)S(1)} %fusion.3) | copy-start | bytes 12582916
  34.7 9.9 %collective-permute-start.5 = (s32[1,2]{1,0:T(1,128)S(1)}, s32[1,2]{1,0:T(1,128)S(1)}, u32[]{:S(2)}, u32[]{:S(2)}) collective-permute-start(s32[1,2]{1,0:T(1,128)S(1)} %get-tuple-element.16), channel_id=1, source_target_pairs={{0,48},{8,56},{16,32},{24,40},{32,16},{40,24},{48,0},{56,8},{64,11... | collective-permute-start | bytes 32 | tf_op jit(solution)/shard_map/ppermute | solution.py:25
  34.7 14.7 %collective-permute-start.6 = (s32[1,2]{1,0:T(1,128)S(1)}, s32[1,2]{1,0:T(1,128)S(1)}, u32[]{:S(2)}, u32[]{:S(2)}) collective-permute-start(s32[1,2]{1,0:T(1,128)S(1)} %get-tuple-element.15), channel_id=1, source_target_pairs={{0,56},{8,48},{16,40},{24,32},{32,24},{40,16},{48,8},{56,0},{64,12... | collective-permute-start | bytes 32 | tf_op jit(solution)/shard_map/ppermute | solution.py:25
  38.4 11.2 %collective-permute-start.7 = (s32[1,2]{1,0:T(1,128)S(1)}, s32[1,2]{1,0:T(1,128)S(1)}, u32[]{:S(2)}, u32[]{:S(2)}) collective-permute-start(s32[1,2]{1,0:T(1,128)S(1)} %get-tuple-element.14), channel_id=1, source_target_pairs={{0,64},{8,72},{16,80},{24,88},{32,96},{40,104},{48,112},{56,120},{... | collective-permute-start | bytes 32 | tf_op jit(solution)/shard_map/ppermute | solution.py:25
  38.6 14.9 %collective-permute-start.8 = (s32[1,2]{1,0:T(1,128)S(1)}, s32[1,2]{1,0:T(1,128)S(1)}, u32[]{:S(2)}, u32[]{:S(2)}) collective-permute-start(s32[1,2]{1,0:T(1,128)S(1)} %get-tuple-element.13), channel_id=1, source_target_pairs={{0,72},{8,64},{16,88},{24,80},{32,104},{40,96},{48,120},{56,112},{... | collective-permute-start | bytes 32 | tf_op jit(solution)/shard_map/ppermute | solution.py:25
  44.3 9.4 %collective-permute-start.9 = (s32[1,2]{1,0:T(1,128)S(1)}, s32[1,2]{1,0:T(1,128)S(1)}, u32[]{:S(2)}, u32[]{:S(2)}) collective-permute-start(s32[1,2]{1,0:T(1,128)S(1)} %get-tuple-element.12), channel_id=1, source_target_pairs={{0,80},{8,88},{16,64},{24,72},{32,112},{40,120},{48,96},{56,104},{... | collective-permute-start | bytes 32 | tf_op jit(solution)/shard_map/ppermute | solution.py:25
  44.5 12.5 %collective-permute-start.10 = (s32[1,2]{1,0:T(1,128)S(1)}, s32[1,2]{1,0:T(1,128)S(1)}, u32[]{:S(2)}, u32[]{:S(2)}) collective-permute-start(s32[1,2]{1,0:T(1,128)S(1)} %get-tuple-element.11), channel_id=1, source_target_pairs={{0,88},{8,80},{16,72},{24,64},{32,120},{40,112},{48,104},{56,96},{... | collective-permute-start | bytes 32 | tf_op jit(solution)/shard_map/ppermute | solution.py:25
  49.4 7.6 %collective-permute-start.11 = (s32[1,2]{1,0:T(1,128)S(1)}, s32[1,2]{1,0:T(1,128)S(1)}, u32[]{:S(2)}, u32[]{:S(2)}) collective-permute-start(s32[1,2]{1,0:T(1,128)S(1)} %get-tuple-element.10), channel_id=1, source_target_pairs={{0,96},{8,104},{16,112},{24,120},{32,64},{40,72},{48,80},{56,88},{... | collective-permute-start | bytes 32 | tf_op jit(solution)/shard_map/ppermute | solution.py:25
  49.6 7.5 %collective-permute-start.12 = (s32[1,2]{1,0:T(1,128)S(1)}, s32[1,2]{1,0:T(1,128)S(1)}, u32[]{:S(2)}, u32[]{:S(2)}) collective-permute-start(s32[1,2]{1,0:T(1,128)S(1)} %get-tuple-element.9), channel_id=1, source_target_pairs={{0,104},{8,96},{16,120},{24,112},{32,72},{40,64},{48,88},{56,80},{... | collective-permute-start | bytes 32 | tf_op jit(solution)/shard_map/ppermute | solution.py:25
  53.5 3.7 %collective-permute-start.13 = (s32[1,2]{1,0:T(1,128)S(1)}, s32[1,2]{1,0:T(1,128)S(1)}, u32[]{:S(2)}, u32[]{:S(2)}) collective-permute-start(s32[1,2]{1,0:T(1,128)S(1)} %get-tuple-element.8), channel_id=1, source_target_pairs={{0,112},{8,120},{16,96},{24,104},{32,80},{40,88},{48,64},{56,72},{... | collective-permute-start | bytes 32 | tf_op jit(solution)/shard_map/ppermute | solution.py:25
  53.7 4.5 %collective-permute-start.14 = (s32[1,2]{1,0:T(1,128)S(1)}, s32[1,2]{1,0:T(1,128)S(1)}, u32[]{:S(2)}, u32[]{:S(2)}) collective-permute-start(s32[1,2]{1,0:T(1,128)S(1)} %get-tuple-element.7), channel_id=1, source_target_pairs={{0,120},{8,112},{16,104},{24,96},{32,88},{40,80},{48,72},{56,64},{... | collective-permute-start | bytes 32 | tf_op jit(solution)/shard_map/ppermute | solution.py:25
  58.4 7.1 %copy-start.8 = (s32[4,4]{1,0:T(4,128)S(1)}, s32[4,4]{1,0:T(4,128)}, u32[]{:S(2)}) copy-start(s32[4,4]{1,0:T(4,128)} %param.27) | copy-start | bytes 196
  58.4 7.2 %copy-start.2 = (bf16[256,2048]{1,0:T(8,128)(2,1)S(1)}, bf16[256,2048]{1,0:T(8,128)(2,1)}, u32[]{:S(2)}) copy-start(bf16[256,2048]{1,0:T(8,128)(2,1)} %param.15) | copy-start | bytes 3145732
  60.1 5.8 %copy-start.7 = (f32[2048]{0:T(1024)S(1)}, f32[2048]{0:T(1024)}, u32[]{:S(2)}) copy-start(f32[2048]{0:T(1024)} %param.16) | copy-start | bytes 24580
  60.1 33.4 %all-to-all-start.1 = ((bf16[16,2,128,128]{3,2,1,0:T(8,128)(2,1)}), bf16[16,2,128,128]{3,2,1,0:T(8,128)(2,1)S(1)}, u32[]{:S(2)}, u32[]{:S(2)}) async-start(bf16[16,2,128,128]{3,2,1,0:T(8,128)(2,1)} %bitcast.13), calls=%async_computation.1 | async-start | bytes 2097152 | tf_op jit(solution)/shard_map/all_to_all | solution.py:115
  65.5 2.1 %copy-start.11 = (bf16[2048,128]{1,0:T(8,128)(2,1)S(1)}, bf16[2048,128]{1,0:T(8,128)(2,1)}, u32[]{:S(2)}) copy-start(bf16[2048,128]{1,0:T(8,128)(2,1)} %param.26) | copy-start | bytes 1572868
  71.1 26.8 %copy-start.5 = (bf16[1,128,128]{2,1,0:T(8,128)(2,1)S(1)}, bf16[1,128,128]{2,1,0:T(8,128)(2,1)}, u32[]{:S(2)}) copy-start(bf16[1,128,128]{2,1,0:T(8,128)(2,1)} %param.19) | copy-start | bytes 98308
  93.4 7.0 %copy-start.3 = (bf16[16,2,128,128]{3,2,1,0:T(8,128)(2,1)}, bf16[16,2,128,128]{3,2,1,0:T(8,128)(2,1)S(1)}, u32[]{:S(2)}) copy-start(bf16[16,2,128,128]{3,2,1,0:T(8,128)(2,1)S(1)} %all-to-all-done.1) | copy-start | bytes 3145732
  93.4 31.5 %all-to-all-start = ((bf16[16,2,128,128]{3,2,1,0:T(8,128)(2,1)}), bf16[16,2,128,128]{3,2,1,0:T(8,128)(2,1)}, u32[]{:S(2)}, u32[]{:S(2)}) async-start(bf16[16,2,128,128]{3,2,1,0:T(8,128)(2,1)} %bitcast.6), calls=%async_computation | async-start | bytes 2097152 | tf_op jit(solution)/shard_map/all_to_all | solution.py:116
  97.9 2.6 %copy-start.9 = (bf16[2048,192]{0,1:T(8,128)(2,1)S(1)}, bf16[2048,192]{0,1:T(8,128)(2,1)}, u32[]{:S(2)}) copy-start(bf16[2048,192]{0,1:T(8,128)(2,1)} %param.21) | copy-start | bytes 2359300
  129.8 2.0 %copy-start.4 = (bf16[128,2048]{1,0:T(8,128)(2,1)S(1)}, bf16[128,2048]{1,0:T(8,128)(2,1)}, u32[]{:S(2)}) copy-start(bf16[128,2048]{1,0:T(8,128)(2,1)} %param.29) | copy-start | bytes 1572868
